TPU v7x, 32 devices: a whole 2x2x4 slice. The times are simulated.
32 devices in a mesh: ep: 8 (over z, y), tp: 4 (over x, core).
Axes of the slice: x: 2, y: 2, z: 4, core: 2. Of those that a mesh axis runs over, the one named last changes fastest.
Arguments:
- tokens: bfloat16 [256, 2048], P('ep'), may hold values from -6 to 6
- gain_mix: bfloat16 [2048], replicated, may hold values from 0.099609375 to 1.8984375
- gain_ffn: bfloat16 [2048], replicated, may hold values from 0.099609375 to 1.8984375
- w_query: bfloat16 [2048, 1024], P('ep', 'tp'), may hold values from -0.125 to 0.125
- w_key: bfloat16 [2048, 1024], P('ep', 'tp'), may hold values from -0.125 to 0.125
- w_value: bfloat16 [2048, 1024], P('ep', 'tp'), may hold values from -0.125 to 0.125
- w_outgate: bfloat16 [2048, 1024], P('ep', 'tp'), may hold values from -0.125 to 0.125
- w_ingate: bfloat16 [2048, 8], replicated, may hold values from -0.125 to 0.125
- w_forget: bfloat16 [2048, 8], replicated, may hold values from -0.125 to 0.125
- bias_in: float32 [8], replicated, may hold values from -2 to 2
- bias_forget: float32 [8], replicated, may hold values from -1 to 3
- w_proj: bfloat16 [1024, 2048], P('tp'), may hold values from -0.1875 to 0.1875
- matrix_state: float32 [256, 8, 128, 128], P('ep', 'tp'), may hold values from -0.6 to 0.6
- normal_state: float32 [256, 8, 128], P('ep', 'tp'), may hold values from -0.6 to 0.6
- stab_state: float32 [256, 8], P('ep', 'tp'), may hold values from -1 to 1
- route_ids: int32 [256, 2], P('ep'), may hold values from 0 to 3, all different within a row; in each aligned block of 32 rows (0 to 31, 32 to 63, ...) at most 32 rows name the same one
- route_weights: float32 [256, 2], P('ep'), may hold values from 0.1 to 1
- w_exp_gate: bfloat16 [8, 2048, 1536], P('ep', None, 'tp'), may hold values from -0.125 to 0.125
- w_exp_up: bfloat16 [8, 2048, 1536], P('ep', None, 'tp'), may hold values from -0.125 to 0.125
- w_exp_down: bfloat16 [8, 1536, 2048], P('ep', 'tp'), may hold values from -0.109375 to 0.109375
Outputs:
- mixed_out: bfloat16 [256, 2048], P('ep', 'tp')
- matrix_out: float32 [256, 8, 128, 128], P('ep', 'tp')
- normal_out: float32 [256, 8, 128], P('ep', 'tp')
- stab_out: float32 [256, 8], P('ep', 'tp')
Inputs may be any that keep to these rules, and one draw needn't show every extreme that they name: `route_ids`: each row names 2 different experts; among the rows of one index of ep no expert is named by more than 32 rows, and in every draw some expert is named by exactly 32 of them.
All inputs are finite; a program needn't handle non-finite values.
Results may differ from a plain program's by a relative error of at most 0.015.
Values may be sent and summed in bfloat16 or wider, within the bound.
A program may use at most 64 MiB of HBM per device.

v0:
```python
import jax
import jax.numpy as jnp
from jax import lax
from jax.sharding import PartitionSpec as P

norm_epsilon = 1e-06


def rms_scale(row_block, gain):
    wide = row_block.astype(jnp.float32)
    factor = lax.rsqrt(jnp.mean(wide * wide, axis=-1, keepdims=True) + norm_epsilon)
    return (wide * factor * gain.astype(jnp.float32)).astype(jnp.bfloat16)


def memory_step(
    query,
    key_rows,
    value_rows,
    gate_rows,
    in_pre,
    forget_pre,
    matrix_state,
    normal_state,
    stab_state,
):
    log_forget = jax.nn.log_sigmoid(forget_pre)
    stab_new = jnp.maximum(log_forget + stab_state, in_pre)
    carry = jnp.exp(log_forget + stab_state - stab_new)
    inflow = jnp.exp(in_pre - stab_new)
    scaled_keys = key_rows.astype(jnp.float32) * query.shape[-1] ** (-0.5)
    value_wide = value_rows.astype(jnp.float32)
    matrix_new = (
        carry[..., None, None] * matrix_state
        + inflow[..., None, None] * scaled_keys[..., :, None] * value_wide[..., None, :]
    )
    normal_new = carry[..., None] * normal_state + inflow[..., None] * scaled_keys
    query_wide = query.astype(jnp.float32)
    numer = jnp.einsum("shd,shde->she", query_wide, matrix_new, precision=lax.Precision.HIGHEST)
    denom = jnp.maximum(jnp.abs(jnp.sum(query_wide * normal_new, axis=-1)), 1.0)
    hidden = numer / denom[..., None] * jax.nn.sigmoid(gate_rows.astype(jnp.float32))
    return (hidden, matrix_new, normal_new, stab_new)


def dispatch_table(route_ids, experts, capacity):
    flat_ids = route_ids.reshape(-1)
    expert_hot = (flat_ids[:, None] == jnp.arange(experts, dtype=jnp.int32)[None, :]).astype(
        jnp.int32
    )
    slot_rank = jnp.sum((jnp.cumsum(expert_hot, axis=0) - 1) * expert_hot, axis=1)
    slot_hot = (slot_rank[:, None] == jnp.arange(capacity, dtype=jnp.int32)[None, :]).astype(
        jnp.float32
    )
    table = expert_hot.astype(jnp.float32)[:, :, None] * slot_hot[:, None, :]
    return table.reshape(flat_ids.shape[0], experts * capacity)


def send_rows(table, row_block, top_count, experts, capacity):
    repeated = jnp.repeat(row_block, top_count, axis=0)
    packed = jnp.einsum(
        "as,aw->sw", table.astype(jnp.bfloat16), repeated, preferred_element_type=jnp.float32
    ).astype(jnp.bfloat16)
    row_width = row_block.shape[1]
    doubled = jnp.broadcast_to(
        packed.reshape(experts, 1, capacity, row_width), (experts, 2, capacity, row_width)
    )
    return doubled.reshape(experts * 2 * capacity, row_width)


def body(
    tokens,
    gain_mix,
    gain_ffn,
    w_query,
    w_key,
    w_value,
    w_outgate,
    w_ingate,
    w_forget,
    bias_in,
    bias_forget,
    w_proj,
    matrix_state,
    normal_state,
    stab_state,
    route_ids,
    route_weights,
    w_exp_gate,
    w_exp_up,
    w_exp_down,
):
    ep_count = lax.axis_size("ep")
    tp_count = lax.axis_size("tp")
    tp_index = lax.axis_index("tp")
    seq_dev = tokens.shape[0]
    model_width = tokens.shape[1]
    heads_dev = matrix_state.shape[1]
    head_dim = matrix_state.shape[2]
    head_cols = w_query.shape[1]
    top_count = route_ids.shape[1]
    experts = ep_count // 2
    capacity = min(seq_dev, max(2, 2 * seq_dev * top_count // experts))
    col_width = model_width // tp_count
    normed = rms_scale(tokens, gain_mix)
    foreign = lax.all_to_all(normed, "ep", split_axis=1, concat_axis=0, tiled=True)
    summed = lax.psum_scatter(
        jnp.concatenate(
            [
                jnp.dot(foreign, weight, preferred_element_type=jnp.float32)
                for weight in (w_query, w_key, w_value, w_outgate)
            ],
            axis=1,
        ),
        "ep",
        scatter_dimension=0,
        tiled=True,
    )
    partials = [summed[:, offset * head_cols : (offset + 1) * head_cols] for offset in range(4)]
    query, key_rows, value_rows, gate_rows = [
        partial_value.astype(jnp.bfloat16).reshape(seq_dev, heads_dev, head_dim)
        for partial_value in partials
    ]
    head_first = tp_index * heads_dev
    in_pre = lax.dynamic_slice_in_dim(
        jnp.dot(normed, w_ingate, preferred_element_type=jnp.float32) + bias_in,
        head_first,
        heads_dev,
        1,
    )
    forget_pre = lax.dynamic_slice_in_dim(
        jnp.dot(normed, w_forget, preferred_element_type=jnp.float32) + bias_forget,
        head_first,
        heads_dev,
        1,
    )
    hidden, matrix_new, normal_new, stab_new = memory_step(
        query,
        key_rows,
        value_rows,
        gate_rows,
        in_pre,
        forget_pre,
        matrix_state,
        normal_state,
        stab_state,
    )
    cell = hidden.reshape(seq_dev, head_cols).astype(jnp.bfloat16)
    partial_out = jnp.dot(cell, w_proj, preferred_element_type=jnp.float32)
    table = dispatch_table(route_ids, experts, capacity)
    gate_local = w_exp_gate[0]
    up_local = w_exp_up[0]
    attended = lax.psum(partial_out.astype(jnp.bfloat16), "tp").astype(jnp.float32)
    resid = (tokens.astype(jnp.float32) + attended).astype(jnp.bfloat16)
    normed_ffn = rms_scale(resid, gain_ffn)
    own_resid = lax.dynamic_slice_in_dim(resid, tp_index * col_width, col_width, 1)
    outgoing = send_rows(table, normed_ffn, top_count, experts, capacity)
    received = lax.all_to_all(outgoing, "ep", split_axis=0, concat_axis=0, tiled=True)
    gate_sum = jnp.dot(received, gate_local, preferred_element_type=jnp.float32)
    up_sum = jnp.dot(received, up_local, preferred_element_type=jnp.float32)
    inner = (jax.nn.silu(gate_sum) * up_sum).astype(jnp.bfloat16)
    expert_terms = jnp.dot(inner, w_exp_down[0], preferred_element_type=jnp.float32)
    half_share = lax.psum_scatter(
        expert_terms.astype(jnp.bfloat16), "tp", scatter_dimension=1, tiled=True
    )
    returned = lax.all_to_all(half_share, "ep", split_axis=0, concat_axis=0, tiled=True)
    halves_summed = jnp.sum(
        returned.astype(jnp.float32).reshape(experts, 2, capacity, col_width), axis=1
    ).reshape(experts * capacity, col_width)
    weights = route_weights / jnp.sum(route_weights, axis=-1, keepdims=True)
    combine = jnp.sum(
        (table * weights.reshape(-1)[:, None]).reshape(seq_dev, top_count, experts * capacity),
        axis=1,
    )
    routed = jnp.dot(combine, halves_summed, precision=lax.Precision.HIGHEST)
    mixed_out = (own_resid.astype(jnp.float32) + routed).astype(jnp.bfloat16)
    return (mixed_out, matrix_new, normal_new, stab_new)


def solution(mesh):
    placed = (
        P("ep", None),
        P(),
        P(),
        P("ep", "tp"),
        P("ep", "tp"),
        P("ep", "tp"),
        P("ep", "tp"),
        P(),
        P(),
        P(),
        P(),
        P("tp", None),
        P("ep", "tp", None, None),
        P("ep", "tp", None),
        P("ep", "tp"),
        P("ep", None),
        P("ep", None),
        P("ep", None, "tp"),
        P("ep", None, "tp"),
        P("ep", "tp", None),
    )
    return jax.shard_map(
        body,
        mesh=mesh,
        in_specs=placed,
        out_specs=(P("ep", "tp"), P("ep", "tp", None, None), P("ep", "tp", None), P("ep", "tp")),
        check_vma=False,
    )
```

profile of v0, /device:TPU:0, one launch (start us, length us, event | category | flops | bytes accessed | tf_op | source)
XLA Modules:
  0.0 213.6 jit_solution(9406941949861868896)
XLA Ops:
  7.2 0.0 copy-start
  7.2 0.0 reduce-scatter.7.cloned.1.call-start
  7.2 1.2 fusion.22
  8.4 0.7 convert_element_type.121
  9.1 1.0 fusion.24
  10.1 14.5 %all_to_all.40 = bf16[32,8,256]{2,0,1:T(8,128)(2,1)S(1)} all-to-all(bf16[32,8,256]{2,0,1:T(8,128)(2,1)S(1)} %bitcast.72), channel_id=1, replica_groups=mesh['ep'=8,'tp'=4] {'ep'}, dimensions={1} | all-to-all | bytes 262144 | tf_op jit(solution)/shard_map/all_to_all | solution.py:104
  24.6 1.1 fusion.41
  25.7 1.1 fusion.40
  26.9 0.2 fusion.39
  27.1 0.2 fusion.38
  27.3 0.1 pad_maximum_fusion
  27.4 0.0 copy-start.10
  27.5 0.0 copy-start.13
  27.5 0.0 copy-start.15
  27.5 1.3 copy.72
  28.8 0.0 reduce-scatter.7.cloned.1.call-update
  28.8 0.0 all-reduce.2.cloned.1.call-start
  28.9 0.1 copy.63
  29.0 0.1 eq.36
  29.1 0.1 fusion.29
  29.2 0.1 copy.64
  29.2 0.1 reduce_window_sum.11
  29.4 0.1 convolution_add_fusion.1
  29.5 0.0 copy-done.13
  29.5 0.1 convolution_add_fusion.2
  29.7 0.0 copy-done.11
  29.7 0.0 copy-start.9
  29.7 0.1 copy.56
  29.8 0.1 copy.57
  29.9 0.2 select_reduce_fusion
  30.1 61.5 %reduce-scatter.7.cloned.1.call-done = f32[32,1024]{1,0:T(8,128)} async-done(((f32[256,1024]{1,0:T(8,128)}), f32[32,1024]{1,0:T(8,128)}) %reduce-scatter.7.cloned.1.call-update) | async-done | bytes 131088
  91.6 1.1 copy.73
  92.7 0.1 copy.60
  92.8 0.1 copy.74
  92.9 0.1 copy.58
  93.0 0.1 copy.59
  93.1 0.8 multiply_reduce_fusion.2
  93.9 0.1 copy.62
  94.0 6.0 %multiply_reduce_fusion = (f32[32,2,128]{2,1,0:T(2,128)S(1)}, f32[32,2,128,128]{3,2,1,0:T(8,128)}) fusion(f32[32,2,128]{2,1,0:T(2,128)S(1)} %copy.74, f32[32,2,128]{2,1,0:T(2,128)S(1)} %copy.59, f32[32,2,128]{2,1,0:T(2,128)S(1)} %get-tuple-element.8, f32[32,2,128,128]{3,2,1,0:T(8,128)} %param.32, f32[32,2]{1,0:T(8,128)S(1)} %copy.56), kind=kLoop, calls=%fused_computation | loop fusion | flops 5234688 | bytes 8519936
  100.0 0.0 copy-start.2
  100.0 0.1 copy.71
  100.1 1.0 convolution_convert_fusion.2
  101.1 0.0 all-reduce.2.cloned.1.call-update
  101.1 0.0 reduce-scatter.5.cloned.1.call-start
  101.2 30.9 %all-reduce.2.cloned.1.call-done = bf16[32,2048]{1,0:T(8,128)(2,1)} async-done(((bf16[32,2048]{1,0:T(8,128)(2,1)}), bf16[32,2048]{1,0:T(8,128)(2,1)}) %all-reduce.2.cloned.1.call-update) | async-done | bytes 131088 | tf_op jit(solution)/shard_map/psum | solution.py:151
  132.1 1.1 fusion.19
  133.1 0.1 fusion.21
  133.3 0.1 broadcast_in_dim.6
  133.4 0.1 reshape.157
  133.5 0.3 convolution_convert_fusion.1
  133.8 0.0 copy-start.1
  133.8 0.1 broadcast_in_dim.8
  133.9 30.2 %all_to_all.41 = bf16[8,32,2048]{2,1,0:T(8,128)(2,1)S(1)} all-to-all(bf16[8,32,2048]{2,1,0:T(8,128)(2,1)S(1)} %bitcast.61), channel_id=1, replica_groups=mesh['ep'=8,'tp'=4] {'ep'}, dimensions={0} | all-to-all | bytes 2097152 | tf_op jit(solution)/shard_map/all_to_all | solution.py:156
  164.1 0.7 fusion.3
  164.9 3.7 %convolution_convert_fusion = bf16[256,2048]{1,0:T(8,128)(2,1)} fusion(bf16[1,384,2048]{2,1,0:T(8,128)(2,1)S(1)} %copy-done, bf16[256,2048]{1,0:T(8,128)(2,1)S(1)} %bitcast.60, bf16[1,2048,384]{2,1,0:T(8,128)(2,1)} %param.38, f32[256,384]{1,0:T(8,128)S(1)} %fusion.3), kind=kOutput, calls=%fused_computation.2 | convolution fusion | flops 806420480 | bytes 5636096 | tf_op jit(solution)/shard_map/dot_general | solution.py:160
  168.6 0.0 reduce-scatter.5.cloned.1.call-update
  168.6 23.2 %reduce-scatter.5.cloned.1.call-done = bf16[256,512]{1,0:T(8,128)(2,1)} async-done(((bf16[256,2048]{1,0:T(8,128)(2,1)}), bf16[256,512]{1,0:T(8,128)(2,1)}) %reduce-scatter.5.cloned.1.call-update) | async-done | bytes 262160 | tf_op jit(solution)/shard_map/reduce_scatter | solution.py:161
  191.8 5.5 %all-to-all-start.2 = ((bf16[8,32,512]{2,1,0:T(8,128)(2,1)}), bf16[8,32,512]{2,1,0:T(8,128)(2,1)S(1)}, u32[]{:S(2)}, u32[]{:S(2)}) async-start(bf16[8,32,512]{2,1,0:T(8,128)(2,1)} %bitcast.74), calls=%async_computation.3 | async-start | bytes 524288 | tf_op jit(solution)/shard_map/all_to_all | solution.py:164
  197.4 0.1 copy.66
  197.5 0.1 copy.65
  197.6 0.1 mul.171
  197.7 0.1 multiply_reduce_fusion.1
  197.8 8.3 %all-to-all-done.2 = bf16[8,32,512]{2,1,0:T(8,128)(2,1)S(1)} async-done(((bf16[8,32,512]{2,1,0:T(8,128)(2,1)}), bf16[8,32,512]{2,1,0:T(8,128)(2,1)S(1)}, u32[]{:S(2)}, u32[]{:S(2)}) %all-to-all-start.2) | async-done | bytes 262176 | tf_op jit(solution)/shard_map/all_to_all | solution.py:164
  206.2 0.9 fusion.13
  (38 shorter events, 0.3 us)
Async XLA Ops:
  7.2 157.7 %copy-start = (bf16[1,384,2048]{2,1,0:T(8,128)(2,1)S(1)}, bf16[1,384,2048]{2,1,0:T(8,128)(2,1)}, u32[]{:S(2)}) copy-start(bf16[1,384,2048]{2,1,0:T(8,128)(2,1)} %param.39) | copy-start | bytes 4718596
  7.2 19.7 %copy-start.4 = (bf16[256,256]{1,0:T(8,128)(2,1)S(1)}, bf16[256,256]{1,0:T(8,128)(2,1)}, u32[]{:S(2)}) copy-start(bf16[256,256]{1,0:T(8,128)(2,1)} %param.24) | copy-start | bytes 393220
  7.2 19.9 %copy-start.5 = (bf16[256,256]{1,0:T(8,128)(2,1)S(1)}, bf16[256,256]{1,0:T(8,128)(2,1)}, u32[]{:S(2)}) copy-start(bf16[256,256]{1,0:T(8,128)(2,1)} %param.23) | copy-start | bytes 393220
  7.2 84.4 %reduce-scatter.7.cloned.1.call-start = ((), (), s32[]{:S(2)}) async-start(), calls=%async_computation.7 | async-start | bytes 1179648
  27.4 1.5 copy-start.10
  27.4 1.9 copy-start.12
  27.4 1.9 copy-start.14
  27.5 2.0 copy-start.13
  27.5 2.0 copy-start.15
  27.5 2.2 %copy-start.11 = (f32[32,2]{0,1:T(2,128)S(1)}, f32[32,2]{0,1:T(2,128)}, u32[]{:S(2)}) copy-start(f32[32,2]{0,1:T(2,128)} %param.34) | copy-start | bytes 772
  28.8 64.3 %copy-start.6 = (f32[32,2,128]{2,1,0:T(2,128)S(1)}, f32[32,2,128]{2,1,0:T(2,128)}, u32[]{:S(2)}) copy-start(f32[32,2,128]{2,1,0:T(2,128)} %param.33) | copy-start | bytes 98308
  28.8 103.2 %all-reduce.2.cloned.1.call-start = ((), (), s32[]{:S(2)}) async-start(), calls=%async_computation.5 | async-start | bytes 262144 | tf_op jit(solution)/shard_map/psum | solution.py:151
  29.7 70.2 %copy-start.9 = (f32[32,2]{0,1:T(2,128)}, f32[32,2]{0,1:T(2,128)S(1)}, u32[]{:S(2)}) copy-start(f32[32,2]{0,1:T(2,128)S(1)} %get-tuple-element.12) | copy-start | bytes 772
  94.0 6.1 %copy-start.3 = (bf16[256,2048]{1,0:T(8,128)(2,1)S(1)}, bf16[256,2048]{1,0:T(8,128)(2,1)}, u32[]{:S(2)}) copy-start(bf16[256,2048]{1,0:T(8,128)(2,1)} %param.31) | copy-start | bytes 3145732
  99.9 1.2 copy-start.7
  100.0 32.1 %copy-start.2 = (bf16[32,2048]{1,0:T(8,128)(2,1)S(1)}, bf16[32,2048]{1,0:T(8,128)(2,1)}, u32[]{:S(2)}) copy-start(bf16[32,2048]{1,0:T(8,128)(2,1)} %param.20) | copy-start | bytes 393220
  101.1 90.7 %reduce-scatter.5.cloned.1.call-start = ((), (), s32[]{:S(2)}) async-start(), calls=%async_computation.6 | async-start | bytes 1310720 | tf_op jit(solution)/shard_map/reduce_scatter | solution.py:161
  133.8 30.3 %copy-start.1 = (bf16[1,2048,384]{2,1,0:T(8,128)(2,1)S(1)}, bf16[1,2048,384]{2,1,0:T(8,128)(2,1)}, u32[]{:S(2)}) copy-start(bf16[1,2048,384]{2,1,0:T(8,128)(2,1)} %param.37) | copy-start | bytes 4718596
  168.6 28.7 %copy-start.8 = (f32[32,2]{0,1:T(2,128)S(1)}, f32[32,2]{0,1:T(2,128)}, u32[]{:S(2)}) copy-start(f32[32,2]{0,1:T(2,128)} %param.36) | copy-start | bytes 772
  191.8 14.3 %all-to-all-start.2 = ((bf16[8,32,512]{2,1,0:T(8,128)(2,1)}), bf16[8,32,512]{2,1,0:T(8,128)(2,1)S(1)}, u32[]{:S(2)}, u32[]{:S(2)}) async-start(bf16[8,32,512]{2,1,0:T(8,128)(2,1)} %bitcast.74), calls=%async_computation.3 | async-start | bytes 524288 | tf_op jit(solution)/shard_map/all_to_all | solution.py:164
Sparse Core Ops, SparseCore 0:
  29.0 62.5 reduce-scatter.6
  101.2 30.8 all-reduce.1
  168.8 23.0 reduce-scatter.4
where the time goes:
time: 214 us
  waiting for transfers between devices  124 us (58%)
  blocking collectives  44.6 us (21%)
  between operations  14.2 us (7%)
  other arithmetic  11.5 us (5%)
  matrix products  9.5 us (4%)
  starting transfers between devices  5.62 us (3%)
  local copies, waits for them, and re-layouts  4.18 us (2%)
    unnamed x4, waiting for transfers between devices  61.5 us
    psum x1, waiting for transfers between devices, body(): lax.psum(partial_out.astype(jnp.bfloat16), 'tp').astype(jnp.float32)  30.9 us
    all_to_all x1, blocking collectives, body(): lax.all_to_all(outgoing, 'ep', split_axis=0, concat_axis=0, tiled=True)  30.2 us
    reduce_scatter x1, waiting for transfers between devices, body(): lax.psum_scatter(expert_terms.astype(jnp.bfloat16), 'tp', scatter_dimensi...  23.2 us
    all_to_all x1, blocking collectives, body(): lax.all_to_all(normed, 'ep', split_axis=1, concat_axis=0, tiled=True)  14.5 us
    all_to_all x1, waiting for transfers between devices, body(): lax.all_to_all(half_share, 'ep', split_axis=0, concat_axis=0, tiled=True)  8.28 us
    unnamed x1, other arithmetic  5.95 us
    all_to_all x1, starting transfers between devices, body(): lax.all_to_all(half_share, 'ep', split_axis=0, concat_axis=0, tiled=True)  5.5 us
  transfers between devices with their start and end apart: 4, of which 4 were waited for; matrix products, arithmetic and copies ran while one was open for 1% of the time, Pallas kernels for 0%

commit v1 on v0

v1 whole, which is shorter than its diff:
```python
import functools

import jax
import jax.numpy as jnp
from jax import lax
from jax.experimental import pallas as pl
from jax.experimental.pallas import tpu as pltpu
from jax.sharding import PartitionSpec as P

norm_epsilon = 1e-06
MESH = pl.DeviceIdType.MESH


def rms_scale(row_block, gain):
    wide = row_block.astype(jnp.float32)
    factor = lax.rsqrt(jnp.mean(wide * wide, axis=-1, keepdims=True) + norm_epsilon)
    return (wide * factor * gain.astype(jnp.float32)).astype(jnp.bfloat16)


def memory_step(
    query,
    key_rows,
    value_rows,
    gate_rows,
    in_pre,
    forget_pre,
    matrix_state,
    normal_state,
    stab_state,
):
    log_forget = jax.nn.log_sigmoid(forget_pre)
    stab_new = jnp.maximum(log_forget + stab_state, in_pre)
    carry = jnp.exp(log_forget + stab_state - stab_new)
    inflow = jnp.exp(in_pre - stab_new)
    scaled_keys = key_rows.astype(jnp.float32) * query.shape[-1] ** (-0.5)
    value_wide = value_rows.astype(jnp.float32)
    matrix_new = (
        carry[..., None, None] * matrix_state
        + inflow[..., None, None] * scaled_keys[..., :, None] * value_wide[..., None, :]
    )
    normal_new = carry[..., None] * normal_state + inflow[..., None] * scaled_keys
    query_wide = query.astype(jnp.float32)
    numer = jnp.einsum("shd,shde->she", query_wide, matrix_new, precision=lax.Precision.HIGHEST)
    denom = jnp.maximum(jnp.abs(jnp.sum(query_wide * normal_new, axis=-1)), 1.0)
    hidden = numer / denom[..., None] * jax.nn.sigmoid(gate_rows.astype(jnp.float32))
    return (hidden, matrix_new, normal_new, stab_new)


def gather_project_kernel(ep_count, tokens_ref, gain_ref, wq_ref, wk_ref, wv_ref, wo_ref, out_ref,
                          blocks, foreign, terms, landed, s1, r1, s2, r2):
    me = lax.axis_index("ep")

    def peer(step):
        return lax.rem(me + step, ep_count)

    def source(step):
        return lax.rem(me - step + ep_count, ep_count)

    barrier = pltpu.get_barrier_semaphore()

    @pl.loop(1, ep_count)
    def _(step):
        pl.semaphore_signal(barrier, inc=1, device_id={"ep": peer(step)}, device_id_type=MESH)

    depth = wq_ref.shape[0]
    wide = tokens_ref[...].astype(jnp.float32)
    factor = lax.rsqrt(jnp.mean(wide * wide, axis=-1, keepdims=True) + norm_epsilon)
    normed = (wide * factor * gain_ref[...].astype(jnp.float32)).astype(jnp.bfloat16)
    for part in range(ep_count):
        blocks[part] = normed[:, part * depth : (part + 1) * depth]
    pl.semaphore_wait(barrier, ep_count - 1)

    def first(step):
        return pltpu.make_async_remote_copy(
            src_ref=blocks.at[peer(step)], dst_ref=foreign.at[me],
            send_sem=s1.at[step], recv_sem=r1.at[step],
            device_id={"ep": peer(step)}, device_id_type=MESH)

    def first_landing(step):
        return pltpu.make_async_remote_copy(
            src_ref=blocks.at[peer(step)], dst_ref=foreign.at[source(step)],
            send_sem=s1.at[step], recv_sem=r1.at[step],
            device_id={"ep": peer(step)}, device_id_type=MESH)

    def second(index, step):
        return pltpu.make_async_remote_copy(
            src_ref=terms.at[index, peer(step)], dst_ref=landed.at[index, me],
            send_sem=s2.at[index, step], recv_sem=r2.at[index, step],
            device_id={"ep": peer(step)}, device_id_type=MESH)

    def second_landing(index, step):
        return pltpu.make_async_remote_copy(
            src_ref=terms.at[index, peer(step)], dst_ref=landed.at[index, source(step)],
            send_sem=s2.at[index, step], recv_sem=r2.at[index, step],
            device_id={"ep": peer(step)}, device_id_type=MESH)

    @pl.loop(1, ep_count)
    def _(step):
        first(step).start()

    foreign[me] = blocks[me]

    @pl.loop(1, ep_count)
    def _(step):
        first_landing(step).wait_recv()

    rows = tokens_ref.shape[0]
    all_rows = foreign[...].reshape(ep_count * rows, depth)
    for index, weight in enumerate((wq_ref, wk_ref, wv_ref, wo_ref)):
        product = jnp.dot(all_rows, weight[...], preferred_element_type=jnp.float32)
        terms[index] = product.astype(jnp.bfloat16).reshape(ep_count, rows, weight.shape[1])

        @pl.loop(1, ep_count)
        def _(step):
            second(index, step).start()

        landed[index, me] = terms[index, me]

    for index in range(4):
        @pl.loop(1, ep_count)
        def _(step):
            second_landing(index, step).wait_recv()

        out_ref[index] = jnp.sum(landed[index].astype(jnp.float32), axis=0).astype(jnp.bfloat16)

    @pl.loop(1, ep_count)
    def _(step):
        first(step).wait_send()
        for index in range(4):
            second(index, step).wait_send()


def gather_project(tokens, gain, weights):
    ep_count = lax.axis_size("ep")
    rows = tokens.shape[0]
    depth, cols = weights[0].shape
    vmem = pl.BlockSpec(memory_space=pltpu.VMEM)
    return pl.pallas_call(
        functools.partial(gather_project_kernel, ep_count),
        out_shape=jax.ShapeDtypeStruct((4, rows, cols), jnp.bfloat16),
        in_specs=[vmem] * 6,
        out_specs=vmem,
        scratch_shapes=[
            pltpu.VMEM((ep_count, rows, depth), jnp.bfloat16),
            pltpu.VMEM((ep_count, rows, depth), jnp.bfloat16),
            pltpu.VMEM((4, ep_count, rows, cols), jnp.bfloat16),
            pltpu.VMEM((4, ep_count, rows, cols), jnp.bfloat16),
            pltpu.SemaphoreType.DMA((ep_count,)),
            pltpu.SemaphoreType.DMA((ep_count,)),
            pltpu.SemaphoreType.DMA((4, ep_count)),
            pltpu.SemaphoreType.DMA((4, ep_count)),
        ],
        compiler_params=pltpu.CompilerParams(
            collective_id=0, has_side_effects=True, vmem_limit_bytes=40 << 20),
        name="gather_project",
    )(tokens, gain.reshape(1, -1), *weights)


def experts_kernel(ep_count, tp_count, cell_ref, tokens_ref, gain_ref, table_ref, wproj_ref,
                   gate_hbm, up_hbm, down_hbm, out_ref,
                   gate_w, up_w, down_w, attn, attn_in, held, normed, inner, tables,
                   scaled, pair_in, half, half_in, share, share_in,
                   w_sem, as_, ar_, ts_, tr_, cs_, cr_, xs_, xr_, ys_, yr_, zs_, zr_,
                   ps_, pr_, us_, ur_, vs_, vr_):
    e = lax.axis_index("ep")
    t = lax.axis_index("tp")
    rows = tokens_ref.shape[0]
    cw = out_ref.shape[1]
    total = ep_count * rows
    near = t + 1 - 2 * lax.rem(t, 2)
    far = lax.rem(t + 2, tp_count)
    across = near + 2 - 4 * (near // 2)

    def peer(step):
        return lax.rem(e + step, ep_count)

    def source(step):
        return lax.rem(e - step + ep_count, ep_count)

    def remote(src, dst, ssem, rsem, target):
        return pltpu.make_async_remote_copy(
            src_ref=src, dst_ref=dst, send_sem=ssem, recv_sem=rsem,
            device_id=target, device_id_type=MESH)

    barrier = pltpu.get_barrier_semaphore()

    @pl.loop(1, ep_count)
    def _(step):
        pl.semaphore_signal(barrier, inc=1, device_id={"ep": peer(step)}, device_id_type=MESH)

    for step in range(1, tp_count):
        pl.semaphore_signal(barrier, inc=1, device_id={"tp": lax.rem(t + step, tp_count)},
                            device_id_type=MESH)
    loads = [pltpu.make_async_copy(src.at[0], dst, w_sem.at[i]) for i, (src, dst) in enumerate(
        ((gate_hbm, gate_w), (up_hbm, up_w), (down_hbm, down_w)))]
    for load in loads:
        load.start()
    cell = cell_ref[...]
    for quarter in range(tp_count):
        attn[quarter] = jnp.dot(
            cell, wproj_ref[:, quarter * cw : (quarter + 1) * cw],
            preferred_element_type=jnp.float32).astype(jnp.bfloat16)
    pl.semaphore_wait(barrier, ep_count - 1 + tp_count - 1)

    def attn_out(step):
        to = lax.rem(t + step, tp_count)
        return remote(attn.at[to], attn_in.at[t], as_.at[step], ar_.at[step], {"tp": to})

    def attn_land(step):
        to = lax.rem(t + step, tp_count)
        frm = lax.rem(t - step + tp_count, tp_count)
        return remote(attn.at[to], attn_in.at[frm], as_.at[step], ar_.at[step], {"tp": to})

    for step in range(1, tp_count):
        attn_out(step).start()
    attn_in[t] = attn[t]

    def table_out(step):
        return remote(table_ref, tables.at[e], ts_.at[step], tr_.at[step], {"ep": peer(step)})

    def table_land(step):
        return remote(table_ref, tables.at[source(step)], ts_.at[step], tr_.at[step],
                      {"ep": peer(step)})

    for step in range(1, tp_count):
        attn_land(step).wait_recv()
    attended = jnp.sum(attn_in[...].astype(jnp.float32), axis=0)
    own_tokens = tokens_ref[:, pl.ds(pl.multiple_of(t * cw, cw), cw)].astype(jnp.float32)
    held[e, t] = (own_tokens + attended).astype(jnp.bfloat16)

    def row_out(step):
        return remote(held.at[e, t], held.at[e, t], cs_.at[step], cr_.at[step],
                      {"ep": peer(step)})

    def row_land(step):
        return remote(held.at[e, t], held.at[source(step), t], cs_.at[step], cr_.at[step],
                      {"ep": peer(step)})

    def far_out(step):
        s = source(step)
        return remote(held.at[s, t], held.at[s, t], xs_.at[step], xr_.at[step], {"tp": far})

    def far_land(step):
        s = source(step)
        return remote(held.at[s, t], held.at[s, far], xs_.at[step], xr_.at[step], {"tp": far})

    def near_out(step):
        s = source(step)
        return remote(held.at[s, t], held.at[s, t], ys_.at[step], yr_.at[step], {"tp": near})

    def near_land(step):
        s = source(step)
        return remote(held.at[s, t], held.at[s, near], ys_.at[step], yr_.at[step], {"tp": near})

    def relay_out(step):
        s = source(step)
        return remote(held.at[s, far], held.at[s, far], zs_.at[step], zr_.at[step], {"tp": near})

    def relay_land(step):
        s = source(step)
        return remote(held.at[s, far], held.at[s, across], zs_.at[step], zr_.at[step],
                      {"tp": near})

    @pl.loop(1, ep_count)
    def _(step):
        row_out(step).start()

    far_out(0).start()
    near_out(0).start()

    @pl.loop(1, ep_count)
    def _(step):
        table_out(step).start()

    tables[e] = table_ref[...]

    @pl.loop(1, ep_count)
    def _(step):
        row_land(step).wait_recv()
        far_out(step).start()
        near_out(step).start()

    @pl.loop(0, ep_count)
    def _(step):
        far_land(step).wait_recv()
        relay_out(step).start()

    @pl.loop(0, ep_count)
    def _(step):
        near_land(step).wait_recv()
        relay_land(step).wait_recv()
        s = source(step)
        parts = [held[s, quarter].astype(jnp.float32) for quarter in range(tp_count)]
        square = sum(jnp.sum(part * part, axis=-1, keepdims=True) for part in parts)
        factor = lax.rsqrt(square / (cw * tp_count) + norm_epsilon)
        for quarter in range(tp_count):
            gain = gain_ref[:, quarter * cw : (quarter + 1) * cw].astype(jnp.float32)
            normed[pl.ds(pl.multiple_of(s * rows, rows), rows), quarter * cw : (quarter + 1) * cw] = (
                parts[quarter] * factor * gain).astype(jnp.bfloat16)

    @pl.loop(1, ep_count)
    def _(step):
        table_land(step).wait_recv()

    loads[0].wait()
    loads[1].wait()
    owners = min(8, ep_count)
    chunk = owners * rows
    chunks = total // chunk

    @pl.loop(0, chunks)
    def _(index):
        window = pl.ds(pl.multiple_of(index * chunk, chunk), chunk)
        block = normed[window, :]
        gate_sum = jnp.dot(block, gate_w[...], preferred_element_type=jnp.float32)
        up_sum = jnp.dot(block, up_w[...], preferred_element_type=jnp.float32)
        inner[window, :] = (gate_sum * jax.nn.sigmoid(gate_sum) * up_sum).astype(jnp.bfloat16)

    loads[2].wait()

    def down(quarter):
        @pl.loop(0, chunks)
        def _(index):
            window = pl.ds(pl.multiple_of(index * chunk, chunk), chunk)
            group = pl.ds(index * owners, owners)
            product = jnp.dot(
                inner[window, :], down_w[:, pl.ds(pl.multiple_of(quarter * cw, cw), cw)],
                preferred_element_type=jnp.float32)
            lanes = lax.broadcasted_iota(jnp.int32, (owners, rows, table_ref.shape[1]), 2)
            weight = jnp.sum(jnp.where(lanes == e // 2, tables[group], 0.0), axis=-1, keepdims=True)
            scaled[quarter, group] = (product.reshape(owners, rows, cw) * weight).astype(
                jnp.bfloat16)

    pair_far = remote(scaled.at[across], pair_in.at[1], ps_.at[1], pr_.at[1], {"tp": near})
    pair_own = remote(scaled.at[near], pair_in.at[0], ps_.at[0], pr_.at[0], {"tp": near})
    down(across)
    pair_far.start()
    down(far)
    down(near)
    pair_own.start()

    def half_out(step):
        p = peer(step)
        return remote(half.at[p], half_in.at[p], us_.at[step], ur_.at[step], {"tp": far})

    def share_out(step):
        return remote(share.at[peer(step)], share_in.at[e], vs_.at[step], vr_.at[step],
                      {"ep": peer(step)})

    def share_land(step):
        return remote(share.at[peer(step)], share_in.at[source(step)], vs_.at[step],
                      vr_.at[step], {"ep": peer(step)})

    pair_far.wait_recv()

    def send_half(step):
        p = peer(step)
        half[p] = (scaled[far, p].astype(jnp.float32) + pair_in[1, p].astype(jnp.float32)).astype(
            jnp.bfloat16)
        half_out(step).start()

    pl.loop(1, ep_count)(send_half)
    send_half(0)
    down(t)
    pair_own.wait_recv()

    def reduced(step):
        p = peer(step)
        half_out(step).wait_recv()
        return (scaled[t, p].astype(jnp.float32) + pair_in[0, p].astype(jnp.float32)
                + half_in[p].astype(jnp.float32)).astype(jnp.bfloat16)

    @pl.loop(1, ep_count)
    def _(step):
        share[peer(step)] = reduced(step)
        share_out(step).start()

    share_in[e] = reduced(0)

    @pl.loop(1, ep_count)
    def _(step):
        share_land(step).wait_recv()

    routed = jnp.sum(share_in[...].astype(jnp.float32), axis=0)
    out_ref[...] = (held[e, t].astype(jnp.float32) + routed).astype(jnp.bfloat16)

    for step in range(1, tp_count):
        attn_out(step).wait_send()
    pair_far.wait_send()
    pair_own.wait_send()

    @pl.loop(1, ep_count)
    def _(step):
        table_out(step).wait_send()
        row_out(step).wait_send()
        share_out(step).wait_send()

    @pl.loop(0, ep_count)
    def _(step):
        far_out(step).wait_send()
        near_out(step).wait_send()
        relay_out(step).wait_send()
        half_out(step).wait_send()


def run_experts(cell, tokens, gain, table, w_proj, w_gate, w_up, w_down):
    ep_count = lax.axis_size("ep")
    tp_count = lax.axis_size("tp")
    rows, width = tokens.shape
    cw = width // tp_count
    hidden = w_gate.shape[2]
    bf16 = jnp.bfloat16
    vmem = pl.BlockSpec(memory_space=pltpu.VMEM)
    hbm = pl.BlockSpec(memory_space=pl.ANY)
    dma = pltpu.SemaphoreType.DMA
    block = (ep_count, rows, cw)
    return pl.pallas_call(
        functools.partial(experts_kernel, ep_count, tp_count),
        out_shape=jax.ShapeDtypeStruct((rows, cw), bf16),
        in_specs=[vmem] * 5 + [hbm] * 3,
        out_specs=vmem,
        scratch_shapes=[
            pltpu.VMEM((width, hidden), bf16),
            pltpu.VMEM((width, hidden), bf16),
            pltpu.VMEM((hidden, width), bf16),
            pltpu.VMEM((tp_count, rows, cw), bf16),
            pltpu.VMEM((tp_count, rows, cw), bf16),
            pltpu.VMEM((ep_count, tp_count, rows, cw), bf16),
            pltpu.VMEM((ep_count * rows, width), bf16),
            pltpu.VMEM((ep_count * rows, hidden), bf16),
            pltpu.VMEM((ep_count,) + table.shape, jnp.float32),
            pltpu.VMEM((tp_count,) + block, bf16),
            pltpu.VMEM((2,) + block, bf16),
            pltpu.VMEM(block, bf16),
            pltpu.VMEM(block, bf16),
            pltpu.VMEM(block, bf16),
            pltpu.VMEM(block, bf16),
            dma((3,)),
            dma((tp_count,)), dma((tp_count,)),
        ] + [dma((ep_count,)) for _ in range(12 - 2)] + [dma((2,)), dma((2,))] + [
            dma((ep_count,)) for _ in range(4)],
        compiler_params=pltpu.CompilerParams(
            collective_id=1, has_side_effects=True, vmem_limit_bytes=60 << 20),
        name="run_experts",
    )(cell, tokens, gain.reshape(1, -1), table, w_proj, w_gate, w_up, w_down)


def body(
    tokens,
    gain_mix,
    gain_ffn,
    w_query,
    w_key,
    w_value,
    w_outgate,
    w_ingate,
    w_forget,
    bias_in,
    bias_forget,
    w_proj,
    matrix_state,
    normal_state,
    stab_state,
    route_ids,
    route_weights,
    w_exp_gate,
    w_exp_up,
    w_exp_down,
):
    ep_count = lax.axis_size("ep")
    tp_index = lax.axis_index("tp")
    seq_dev = tokens.shape[0]
    heads_dev = matrix_state.shape[1]
    head_dim = matrix_state.shape[2]
    head_cols = w_query.shape[1]
    experts = ep_count // 2
    normed = rms_scale(tokens, gain_mix)
    projected = gather_project(tokens, gain_mix, (w_query, w_key, w_value, w_outgate))
    query, key_rows, value_rows, gate_rows = [
        projected[index].reshape(seq_dev, heads_dev, head_dim) for index in range(4)
    ]
    head_first = tp_index * heads_dev
    in_pre = lax.dynamic_slice_in_dim(
        jnp.dot(normed, w_ingate, preferred_element_type=jnp.float32) + bias_in,
        head_first,
        heads_dev,
        1,
    )
    forget_pre = lax.dynamic_slice_in_dim(
        jnp.dot(normed, w_forget, preferred_element_type=jnp.float32) + bias_forget,
        head_first,
        heads_dev,
        1,
    )
    hidden, matrix_new, normal_new, stab_new = memory_step(
        query,
        key_rows,
        value_rows,
        gate_rows,
        in_pre,
        forget_pre,
        matrix_state,
        normal_state,
        stab_state,
    )
    cell = hidden.reshape(seq_dev, head_cols).astype(jnp.bfloat16)
    weights = route_weights / jnp.sum(route_weights, axis=-1, keepdims=True)
    lanes = -(-experts // 128) * 128
    named = route_ids[:, :, None] == jnp.arange(lanes, dtype=jnp.int32)[None, None, :]
    table = jnp.sum(jnp.where(named, weights[:, :, None], 0.0), axis=1)
    mixed_out = run_experts(
        cell, tokens, gain_ffn, table, w_proj, w_exp_gate, w_exp_up, w_exp_down
    )
    return (mixed_out, matrix_new, normal_new, stab_new)


def solution(mesh):
    placed = (
        P("ep", None),
        P(),
        P(),
        P("ep", "tp"),
        P("ep", "tp"),
        P("ep", "tp"),
        P("ep", "tp"),
        P(),
        P(),
        P(),
        P(),
        P("tp", None),
        P("ep", "tp", None, None),
        P("ep", "tp", None),
        P("ep", "tp"),
        P("ep", None),
        P("ep", None),
        P("ep", None, "tp"),
        P("ep", None, "tp"),
        P("ep", "tp", None),
    )
    return jax.shard_map(
        body,
        mesh=mesh,
        in_specs=placed,
        out_specs=(P("ep", "tp"), P("ep", "tp", None, None), P("ep", "tp", None), P("ep", "tp")),
        check_vma=False,
    )
```

time: 214 us -> 83.4 us (0.39)
  waiting for transfers between devices: 124 us -> 0 us
  Pallas kernels: 0 us -> 59.2 us
  blocking collectives: 44.6 us -> 0 us
  between operations: 14.2 us -> 0.78 us
  local copies, waits for them, and re-layouts: 4.18 us -> 10.1 us
  starting transfers between devices: 5.62 us -> 0 us
  matrix products: 9.5 us -> 4.29 us
  other arithmetic: 11.5 us -> 8.52 us
    unnamed x4 -> x0, waiting for transfers between devices: 61.5 us -> none
    pallas_call x0 -> x2, Pallas kernels: none -> 59.2 us  [the longest x1 35.7 us: run_experts(): pl.pallas_call(functools.partial(experts_kernel, ep_count, tp_count), out...]
    all_to_all x2 -> x0, blocking collectives: 44.6 us -> none  [the longest x1 30.2 us: body(): lax.all_to_all(outgoing, 'ep', split_axis=0, concat_axis=0, tiled=True)]
    psum x1 -> x0, waiting for transfers between devices: 30.9 us -> none  [body(): lax.psum(partial_out.astype(jnp.bfloat16), 'tp').astype(jnp.float32)]
    reduce_scatter x1 -> x0, waiting for transfers between devices: 23.2 us -> none  [body(): lax.psum_scatter(expert_terms.astype(jnp.bfloat16), 'tp', scatter_dimensi...]
    all_to_all x1 -> x0, waiting for transfers between devices: 8.28 us -> none  [body(): lax.all_to_all(half_share, 'ep', split_axis=0, concat_axis=0, tiled=True)]
    dot_general x9 -> x1, matrix products: 9.29 us -> 2.01 us  [memory_step(): jnp.einsum('shd,shde->she', query_wide, matrix_new, precision=lax.Precisi...]
    unnamed x1 -> x0, other arithmetic: 5.95 us -> none
  transfers between devices with their start and end apart: 4 -> 0, of which waited for: 4 -> 0; matrix products, arithmetic and copies ran while one was open for 1% -> 0% of each run, Pallas kernels for 0% -> 0%
where the time goes in v1:
time: 83.4 us; the launch traced here: 82.8 us
  Pallas kernels  59.2 us (71%)
  local copies, waits for them, and re-layouts  10.1 us (12%)
  other arithmetic  8.52 us (10%)
  matrix products  4.29 us (5%)
    pallas_call x1, Pallas kernels, run_experts(): pl.pallas_call(functools.partial(experts_kernel, ep_count, tp_count), out...  35.7 us
    pallas_call x1, Pallas kernels, gather_project(): pl.pallas_call(functools.partial(gather_project_kernel, ep_count), out_sh...  23.5 us
    unnamed x24, local copies, waits for them, and re-layouts  8.54 us
    add x1, other arithmetic, memory_step(): carry[..., None, None] * matrix_state  3.69 us
    dot_general x1, matrix products, memory_step(): jnp.einsum('shd,shde->she', query_wide, matrix_new, precision=lax.Precisi...  2.01 us

profile of v1, /device:TPU:0, one launch (start us, length us, event | category | flops | bytes accessed | tf_op | source)
XLA Modules:
  0.0 82.8 jit_solution(4325223457765745975)
XLA Ops:
  0.6 0.0 copy-start
  0.6 0.7 reshape.61.gain_ref
  1.3 0.0 copy-start.1
  1.3 0.9 %copy-done.1 = bf16[32,2048]{1,0:T(8,128)(2,1)S(1)} copy-done((bf16[32,2048]{1,0:T(8,128)(2,1)S(1)}, bf16[32,2048]{1,0:T(8,128)(2,1)}, u32[]{:S(2)}) %copy-start.1) | copy-done | bytes 131096
  2.2 0.0 copy-start.2
  2.3 0.9 %copy-done.2 = bf16[256,256]{1,0:T(8,128)(2,1)S(1)} copy-done((bf16[256,256]{1,0:T(8,128)(2,1)S(1)}, bf16[256,256]{1,0:T(8,128)(2,1)}, u32[]{:S(2)}) %copy-start.2) | copy-done | bytes 131096
  3.2 0.0 copy-start.3
  3.2 0.9 %copy-done.3 = bf16[256,256]{1,0:T(8,128)(2,1)S(1)} copy-done((bf16[256,256]{1,0:T(8,128)(2,1)S(1)}, bf16[256,256]{1,0:T(8,128)(2,1)}, u32[]{:S(2)}) %copy-start.3) | copy-done | bytes 131096
  4.1 0.0 copy-start.4
  4.1 0.9 %copy-done.4 = bf16[256,256]{1,0:T(8,128)(2,1)S(1)} copy-done((bf16[256,256]{1,0:T(8,128)(2,1)S(1)}, bf16[256,256]{1,0:T(8,128)(2,1)}, u32[]{:S(2)}) %copy-start.4) | copy-done | bytes 131096
  5.0 0.0 copy-start.5
  5.0 0.9 %copy-done.5 = bf16[256,256]{1,0:T(8,128)(2,1)S(1)} copy-done((bf16[256,256]{1,0:T(8,128)(2,1)S(1)}, bf16[256,256]{1,0:T(8,128)(2,1)}, u32[]{:S(2)}) %copy-start.5) | copy-done | bytes 131096
  5.9 23.5 %gather_project.1 = bf16[4,32,256]{2,1,0:T(8,128)(2,1)S(1)} custom-call(bf16[32,2048]{1,0:T(8,128)(2,1)S(1)} %copy-done.1, bf16[1,2048]{1,0:T(2,128)(2,1)S(1)} %reshape.61.gain_ref, bf16[256,256]{1,0:T(8,128)(2,1)S(1)} %copy-done.2, bf16[256,256]{1,0:T(8,128)(2,1)S(1)} %copy-done.3, bf16[256,256]{1,0:T(8,128)(2,1)S(1)} %copy-done.4, ...), custom_call_target="tpu_custom_call" | custom-call | tf_op jit(solution)/shard_map/gather_project/pallas_call | solution.py:138
  29.5 0.7 convert_element_type.42
  30.2 1.0 %fusion = f32[32]{0:T(128)S(1)} fusion(bf16[32,2048]{1,0:T(8,128)(2,1)} %tokens_ref.3), kind=kLoop, calls=%fused_computation.5 | loop fusion | flops 196576 | bytes 131200 | tf_op jit(solution)/shard_map/reduce_sum | solution.py:16
  31.2 0.0 copy-done
  31.3 1.1 %convolution_add_fusion = f32[32,8]{0,1:T(8,128)S(1)} fusion(bf16[2048,8]{0,1:T(8,128)(2,1)S(1)} %copy-done, bf16[32,2048]{1,0:T(8,128)(2,1)} %tokens_ref.3, f32[2048]{0:T(1024)S(1)} %convert_element_type.42, f32[32]{0:T(128)S(1)} %add_rsqrt_fusion, f32[8]{0:T(128)} %param.29), kind=kOutput, calls=%fused_computation.1 | convolution fusion | flops 1310976 | bytes 173216 | tf_op jit(solution)/shard_map/dot_general | solution.py:484
  32.4 1.1 %convolution_add_fusion.1 = f32[32,8]{0,1:T(8,128)S(1)} fusion(bf16[2048,8]{0,1:T(8,128)(2,1)} %param.28, bf16[32,2048]{1,0:T(8,128)(2,1)} %tokens_ref.3, f32[2048]{0:T(1024)S(1)} %convert_element_type.42, f32[32]{0:T(128)S(1)} %add_rsqrt_fusion, f32[8]{0:T(128)} %param.30), kind=kOutput, calls=%fused_computation.2 | convolution fusion | flops 1310976 | bytes 173216 | tf_op jit(solution)/shard_map/dot_general | solution.py:490
  33.5 0.7 subtract_exponential_fusion
  34.2 0.0 copy-start.9
  34.2 0.1 copy.29
  34.4 0.1 copy.30
  34.5 1.5 %multiply_reduce_fusion = (f32[32,2]{1,0:T(8,128)S(1)}, f32[32,2,128]{2,1,0:T(2,128)}, f32[32,2,128]{2,1,0:T(2,128)S(1)}) fusion(bf16[32,2,128]{2,1,0:T(2,128)(2,1)S(1)} %reshape_squeeze.2, f32[32,2,128]{2,1,0:T(2,128)} %param.33, f32[32,2]{1,0:T(8,128)S(1)} %copy.29, f32[32,2,128]{2,1,0:T(2,128)S(1)} %reshape.63, f32[32,2]{1,0:T(8,128)S(1)} %copy.30), kind=kLoop, calls=%fused_computation.12 | loop fusion | flops 49088 | bytes 148224 | tf_op jit(solution)/shard_map/reduce_sum | solution.py:44
  36.0 3.7 %multiply_add_fusion = f32[32,2,128,128]{3,2,1,0:T(8,128)S(1)} fusion(f32[32,2,128,128]{3,2,1,0:T(8,128)} %param.32, f32[32,2,128]{2,1,0:T(2,128)S(1)} %reshape.64, f32[32,2,128]{2,1,0:T(2,128)S(1)} %get-tuple-element.6, f32[32,2]{1,0:T(8,128)S(1)} %copy.29), kind=kLoop, calls=%fused_computation | loop fusion | flops 3145728 | bytes 8454400 | tf_op jit(solution)/shard_map/add | solution.py:38
  39.7 0.0 copy-done.9
  39.7 0.0 copy-start.6
  39.7 2.0 %copy-done.6 = f32[32,2,128,128]{3,2,1,0:T(8,128)} copy-done((f32[32,2,128,128]{3,2,1,0:T(8,128)}, f32[32,2,128,128]{3,2,1,0:T(8,128)S(1)}, u32[]{:S(2)}) %copy-start.6) | copy-done | bytes 4194328
  41.7 0.0 copy-start.7
  41.7 0.0 copy-start.8
  41.7 0.0 copy-start.10
  41.7 2.0 %fusion.8 = f32[32,2,1,128]{3,2,1,0:T(1,128)S(1)} fusion(bf16[32,2,128,1]{2,3,1,0:T(2,128)(2,1)S(1)} %reshape.70, f32[32,2,128,128]{3,2,1,0:T(8,128)S(1)} %multiply_add_fusion), kind=kOutput, calls=%fused_computation.28 | convolution fusion | flops 12582912 | bytes 4243456 | tf_op jit(solution)/shard_map/shd,shde->she/dot_general | solution.py:43
  43.7 0.1 fusion.5
  43.9 0.6 copy.36
  44.5 0.0 copy-done.7
  44.5 0.6 reshape.62.gain_ref
  45.1 0.0 copy-done.8
  45.1 0.0 copy-done.10
  45.1 0.7 select_reduce_fusion.table_ref
  45.8 35.7 %run_experts.1 = bf16[32,512]{1,0:T(8,128)(2,1)} custom-call(bf16[32,256]{1,0:T(8,128)(2,1)} %bitcast.11, bf16[32,2048]{1,0:T(8,128)(2,1)} %tokens_ref.3, bf16[1,2048]{1,0:T(2,128)(2,1)} %reshape.62.gain_ref, f32[32,128]{1,0:T(8,128)} %select_reduce_fusion.table_ref, bf16[256,2048]{1,0:T(8,128)(2,1)} %wproj_ref.1, bf16[1,2048,384]{2,1,0:T(8,128)(2,1)} %gate_hbm.1, ...), custom_call_target="tpu_custom_call" | custom-call | tf_op jit(solution)/shard_map/run_experts/pallas_call | solution.py:417
  81.5 1.4 %copy.38 = bf16[32,512]{1,0:T(8,128)(2,1)} copy(bf16[32,512]{1,0:T(8,128)(2,1)} %run_experts.1) | data formatting | bytes 65536
  (12 shorter events, 0.2 us)
Async XLA Ops:
  0.6 30.6 %copy-start = (bf16[2048,8]{0,1:T(8,128)(2,1)S(1)}, bf16[2048,8]{0,1:T(8,128)(2,1)}, u32[]{:S(2)}) copy-start(bf16[2048,8]{0,1:T(8,128)(2,1)} %param.27) | copy-start | bytes 98308
  1.3 0.9 %copy-start.1 = (bf16[32,2048]{1,0:T(8,128)(2,1)S(1)}, bf16[32,2048]{1,0:T(8,128)(2,1)}, u32[]{:S(2)}) copy-start(bf16[32,2048]{1,0:T(8,128)(2,1)} %tokens_ref.3) | copy-start | bytes 393220
  2.2 0.9 %copy-start.2 = (bf16[256,256]{1,0:T(8,128)(2,1)S(1)}, bf16[256,256]{1,0:T(8,128)(2,1)}, u32[]{:S(2)}) copy-start(bf16[256,256]{1,0:T(8,128)(2,1)} %wq_ref.1) | copy-start | bytes 393220
  3.2 0.9 %copy-start.3 = (bf16[256,256]{1,0:T(8,128)(2,1)S(1)}, bf16[256,256]{1,0:T(8,128)(2,1)}, u32[]{:S(2)}) copy-start(bf16[256,256]{1,0:T(8,128)(2,1)} %wk_ref.1) | copy-start | bytes 393220
  4.1 0.9 %copy-start.4 = (bf16[256,256]{1,0:T(8,128)(2,1)S(1)}, bf16[256,256]{1,0:T(8,128)(2,1)}, u32[]{:S(2)}) copy-start(bf16[256,256]{1,0:T(8,128)(2,1)} %wv_ref.1) | copy-start | bytes 393220
  5.0 0.9 %copy-start.5 = (bf16[256,256]{1,0:T(8,128)(2,1)S(1)}, bf16[256,256]{1,0:T(8,128)(2,1)}, u32[]{:S(2)}) copy-start(bf16[256,256]{1,0:T(8,128)(2,1)} %wo_ref.1) | copy-start | bytes 393220
  34.2 5.4 %copy-start.9 = (f32[32,2]{0,1:T(2,128)}, f32[32,2]{0,1:T(2,128)S(1)}, u32[]{:S(2)}) copy-start(f32[32,2]{0,1:T(2,128)S(1)} %get-tuple-element.19) | copy-start | bytes 772
  39.7 2.0 %copy-start.6 = (f32[32,2,128,128]{3,2,1,0:T(8,128)}, f32[32,2,128,128]{3,2,1,0:T(8,128)S(1)}, u32[]{:S(2)}) copy-start(f32[32,2,128,128]{3,2,1,0:T(8,128)S(1)} %multiply_add_fusion) | copy-start | bytes 12582916
  41.7 2.8 %copy-start.7 = (bf16[2048]{0:T(1024)(128)(2,1)S(1)}, bf16[2048]{0:T(1024)(128)(2,1)}, u32[]{:S(2)}) copy-start(bf16[2048]{0:T(1024)(128)(2,1)} %param.22) | copy-start | bytes 12292
  41.7 3.4 %copy-start.8 = (f32[32,2]{0,1:T(2,128)S(1)}, f32[32,2]{0,1:T(2,128)}, u32[]{:S(2)}) copy-start(f32[32,2]{0,1:T(2,128)} %param.36) | copy-start | bytes 772
  41.7 3.4 %copy-start.10 = (s32[32,2]{0,1:T(2,128)S(1)}, s32[32,2]{0,1:T(2,128)}, u32[]{:S(2)}) copy-start(s32[32,2]{0,1:T(2,128)} %param.35) | copy-start | bytes 772
